TPU v7x, 32 devices: a whole 2x2x4 slice. The times are simulated.
32 devices in a mesh: gr: 2 (over x), fs: 8 (over z, y), tp: 2 (over core).
Axes of the slice: x: 2, y: 2, z: 4, core: 2. Of those that a mesh axis runs over, the one named last changes fastest.
Arguments:
- tokens: bfloat16 [4096, 2048], P(('gr', 'fs', 'tp')), may hold values from -6 to 6
- norm_gain: float32 [2048], P(('gr', 'fs')), may hold values from 0.1 to 1.9
- up_weight: float32 [2048, 8192], P(('gr', 'fs'), 'tp'), may hold values from -0.125 to 0.125
- down_weight: float32 [8192, 2048], P(('gr', 'fs'), 'tp'), may hold values from -0.0625 to 0.0625
Outputs:
- served: bfloat16 [4096, 2048], P(('gr', 'fs', 'tp'))
- serve_up: bfloat16 [2048, 8192], P(None, 'fs')
- serve_down: bfloat16 [8192, 2048], P('fs')
All inputs are finite; a program needn't handle non-finite values.
Results may differ from a plain program's by a relative error of at most 0.017.
Values may be sent and summed in bfloat16 or wider, within the bound.
A program may use at most 64 MiB of HBM per device.

v0:
```python
import functools

import jax
import jax.numpy as jnp
from jax import lax
from jax.experimental import pallas as pl
from jax.experimental.pallas import tpu as pltpu
from jax.sharding import PartitionSpec as P

MESH = pl.DeviceIdType.MESH
TILE = 512


def inner_size(shards):
    return max(d for d in range(1, shards + 1) if shards % d == 0 and d * d <= shards)


def kernel(sizes, normed, up, down, served, su, sd, tok, hid, part, got, far, *sems):
    groups, shards, cores = sizes
    inner = inner_size(shards)
    outer = shards // inner
    (up_send, up_recv, gu_send, gu_recv, tu_send, tu_recv, gd_send, gd_recv,
     td_send, td_recv, tok_send, tok_recv, part_send, part_recv, far_send, far_recv, hop_send, ou_send, ou_recv, local) = sems
    g, f, t = lax.axis_index("gr"), lax.axis_index("fs"), lax.axis_index("tp")
    z, y = f // inner, lax.rem(f, inner)
    rows, depth = normed.shape
    own_rows = up.shape[0]
    segment, dcols = down.shape
    nseg = up.shape[1] // segment
    group_rows = shards * own_rows

    def to(axis, me, size, step):
        return {axis: lax.rem(me + step, size)}

    def rdma(src, dst, send, recv, device):
        return pltpu.make_async_remote_copy(
            src_ref=src, dst_ref=dst, send_sem=send, recv_sem=recv,
            device_id=device, device_id_type=MESH,
        )

    def back(o, i):
        return {"fs": lax.rem(z + outer - o, outer) * inner + lax.rem(y + inner - i, inner)}

    def ahead(o, i):
        return {"fs": lax.rem(z + o, outer) * inner + lax.rem(y + i, inner)}

    def block_of(ref, number, count=1):
        return ref.at[pl.ds(pl.multiple_of(number * rows, rows), count * rows)]

    peers = [to("fs", f, shards, k) for k in range(1, shards)]
    peers += [to("gr", g, groups, k) for k in range(1, groups)]
    peers += [to("tp", t, cores, k) for k in range(1, cores)]
    barrier = pltpu.get_barrier_semaphore()
    for peer in peers:
        pl.semaphore_signal(barrier, inc=1, device_id=peer, device_id_type=MESH)
    pl.semaphore_wait(barrier, len(peers))

    def up_block(group, shard, sg):
        row = pl.multiple_of((group * shards + shard) * own_rows, own_rows)
        return su.at[pl.ds(row, own_rows), pl.ds(pl.multiple_of(sg * segment, segment), segment)]

    def up_group(group, sg):
        row = pl.multiple_of(group * group_rows, group_rows)
        return su.at[pl.ds(row, group_rows), pl.ds(sg * segment, segment)]

    def down_block(group, core):
        row = pl.multiple_of(group * segment, segment)
        return sd.at[pl.ds(row, segment), pl.ds(pl.multiple_of(core * dcols, dcols), dcols)]

    def owner(sg):
        return (sg * shards + f) // nseg

    sends = []
    keep_down = pltpu.make_async_copy(down, down_block(g, t), local.at[0])
    keep_tok = pltpu.make_async_copy(normed, block_of(tok, 0), local.at[1])
    keep_down.start()
    keep_tok.start()
    down_in = []
    for k in range(1, groups):
        copy = rdma(down, down_block(g, t), gd_send.at[k], gd_recv.at[k], to("gr", g, groups, k))
        copy.start()
        sends.append(copy)
        source = lax.rem(g + groups - k, groups)
        down_in.append((k, source))
    for k in range(1, cores):
        copy = rdma(down, down_block(g, t), td_send.at[k, 0], td_recv.at[k, 0], to("tp", t, cores, k))
        copy.start()
        sends.append(copy)

    for i in range(1, inner):
        copy = rdma(normed, block_of(tok, i), tok_send.at[i], tok_recv.at[i], ahead(0, i))
        copy.start()
        sends.append(copy)

    def beside(step):
        return {"fs": (z + step) * inner + y}

    def hop(o, step):
        source = normed if o in (0, outer) else block_of(tok, o * inner)
        n = (o + step) * inner
        return rdma(source, block_of(tok, n), hop_send.at[o + step if step > 0 else outer + o + step], tok_recv.at[n], beside(step))

    low, high = z > 0, z < outer - 1
    hops = []

    def move(o, step, when):
        pl.when(when)(lambda: hop(o, step).start())
        hops.append((o, step, when))

    move(0, 1, high)
    move(outer, -1, low)

    def up_copy(i):
        number = t * nseg + i
        shard, sg = lax.rem(number, shards), number // shards
        step = lax.rem(shard - f + shards, shards)
        src = up.at[:, pl.ds(pl.multiple_of(i * segment, segment), segment)]
        remote = rdma(src, up_block(g, f, sg), up_send.at[i], up_recv.at[sg, step], {"fs": shard})
        here = pltpu.make_async_copy(src, up_block(g, f, sg), up_recv.at[sg, 0])
        return shard == f, here, remote

    def start_up(j, carry):
        mine, here, remote = up_copy(lax.rem(f + j, nseg))
        pl.when(mine)(here.start)
        pl.when(jnp.logical_not(mine))(remote.start)
        return carry

    lax.fori_loop(0, nseg, start_up, 0)

    def pass_on(o):
        for n, when, step, more in ((o, z >= o, 1, high), (outer - o, z + o < outer, -1, low)):
            block = block_of(tok, n * inner)

            @pl.when(when)
            def _(n=n, step=step, block=block):
                rdma(block, block, tok_send.at[0], tok_recv.at[n * inner], beside(-step)).wait_recv()

            if 0 < n + step < outer:
                move(n, step, when & more)

            @pl.when(when)
            def _(n=n, block=block):
                for i in range(1, inner):
                    at = n * inner + i
                    rdma(block, block_of(tok, at), tok_send.at[at], tok_recv.at[at], ahead(0, i)).start()

    if outer > 1:
        pass_on(1)

    for sg in range(groups):
        def forward(sg=sg):
            def arrived(k, carry):
                shard = lax.rem(f + shards - k, shards)
                block = up_block(g, shard, sg)

                @pl.when(k == 0)
                def _():
                    pltpu.make_async_copy(block, block, up_recv.at[sg, 0]).wait()

                @pl.when(k > 0)
                def _():
                    rdma(block, block, up_send.at[0], up_recv.at[sg, k], {"fs": shard}).wait_recv()

                for d in range(1, groups):
                    rdma(block, block, gu_send.at[sg, d, k], gu_recv.at[sg, d, k],
                         to("gr", g, groups, d)).start()
                return carry

            lax.fori_loop(0, shards, arrived, 0)
            whole = up_group(g, sg)
            for c in range(1, cores):
                rdma(whole, whole, tu_send.at[sg, 0, c], tu_recv.at[sg, 0], to("tp", t, cores, c)).start()

        pl.when(owner(sg) == t)(forward)

    for o in range(2, outer):
        pass_on(o)

    for k, source in down_in:
        block = down_block(source, t)
        rdma(block, block, gd_send.at[k], gd_recv.at[k], {"gr": source}).wait_recv()
        for c in range(1, cores):
            copy = rdma(block, block, td_send.at[c, k], td_recv.at[c, k], to("tp", t, cores, c))
            copy.start()
            sends.append(copy)

    for sg in range(groups):
        def onward(sg=sg):
            for d in range(1, groups):
                source = lax.rem(g + groups - d, groups)

                def arrived(k, carry):
                    block = up_block(source, lax.rem(f + shards - k, shards), sg)
                    rdma(block, block, gu_send.at[sg, d, k], gu_recv.at[sg, d, k], {"gr": source}).wait()
                    for c in range(1, cores):
                        rdma(block, block, ou_send.at[sg, d, c, k], ou_recv.at[sg, d, k],
                             to("tp", t, cores, c)).start()
                    return carry

                lax.fori_loop(0, shards, arrived, 0)

        pl.when(owner(sg) == t)(onward)

    keep_down.wait()
    keep_tok.wait()
    for c in range(1, cores):
        core = lax.rem(t + cores - c, cores)
        for k in range(groups):
            block = down_block(lax.rem(g + groups - k, groups), core)
            rdma(block, block, td_send.at[c, k], td_recv.at[c, k], {"tp": core}).wait_recv()
    for sg in range(groups):
        def take(sg=sg):
            whole = up_group(g, sg)
            rdma(whole, whole, tu_send.at[sg, 0, 1], tu_recv.at[sg, 0], {"tp": owner(sg)}).wait_recv()
            for d in range(1, groups):
                def taken(k, carry):
                    block = up_block(lax.rem(g + groups - d, groups), lax.rem(f + shards - k, shards), sg)
                    rdma(block, block, tu_send.at[sg, 0, 1], ou_recv.at[sg, d, k],
                         {"tp": owner(sg)}).wait_recv()
                    return carry

                lax.fori_loop(0, shards, taken, 0)

        pl.when(owner(sg) != t)(take)

    width = su.shape[1]
    stack = inner * rows

    def near_copy(o, i):
        n = o * inner + i
        return rdma(block_of(part, n), block_of(got, n), part_send.at[n], part_recv.at[n], back(0, i))

    def far_copy(o):
        right = o > z
        step = jnp.where(right, 1, -1)
        last = jnp.where(right, o == outer - 1, o == 1)
        slot = jnp.where(last, jnp.where(right, 0, outer), o + step)
        return rdma(block_of(part, o * inner), block_of(far, slot), far_send.at[o], far_recv.at[slot],
                    beside(step))

    def far_arrived(slot, step):
        rdma(block_of(far, slot), block_of(far, slot), far_send.at[0], far_recv.at[slot],
             beside(step)).wait_recv()

    def compute(o):
        for i in range(1, inner):
            block = block_of(tok, o * inner + i)
            n = o * inner + i
            rdma(block, block, tok_send.at[n], tok_recv.at[n], back(0, i)).wait_recv()
        both = pl.ds(pl.multiple_of(o * stack, stack), stack)

        def first(n, carry):
            cols = pl.ds(pl.multiple_of(n * TILE, TILE), TILE)
            product = jnp.dot(tok[both, :], su[:, cols], preferred_element_type=jnp.float32)
            product = jnp.maximum(product, 0.0)
            hid[:, cols] = (product * product).astype(jnp.bfloat16)
            return carry

        lax.fori_loop(0, width // TILE, first, 0)

        def second(n, carry):
            cols = pl.ds(pl.multiple_of(n * TILE, TILE), TILE)
            product = jnp.dot(hid[...], sd[:, cols], preferred_element_type=jnp.float32)
            part[both, cols] = product.astype(jnp.bfloat16)
            return carry

        lax.fori_loop(0, depth // TILE, second, 0)
        for i in range(1, inner):
            near_copy(o, i).start()

    def gather(o):
        for i in range(1, inner):
            near_copy(o, i).wait()

    def add(o):
        gather(o)

        def sum_up(passed):
            def chunk(r, carry):
                at = pl.multiple_of(r * 16, 16)
                mine = pl.ds(pl.multiple_of(o * stack + at, 16), 16)
                value = part[mine, :].astype(jnp.float32)
                for i in range(1, inner):
                    near = pl.ds(pl.multiple_of(o * stack + i * rows + at, 16), 16)
                    value += got[near, :].astype(jnp.float32)
                if passed:
                    value += far[pl.ds(pl.multiple_of(o * rows + at, 16), 16), :].astype(jnp.float32)
                part[mine, :] = value.astype(jnp.bfloat16)
                return carry

            lax.fori_loop(0, rows // 16, chunk, 0)

        right = o > z
        passed = (right & low) | (jnp.logical_not(right) & high)

        @pl.when(passed)
        def _():
            far_arrived(o, jnp.where(right, -1, 1))
            sum_up(True)

        pl.when(jnp.logical_not(passed))(lambda: sum_up(False))
        far_copy(o).start()

    order = []
    left_end, right_end = z * 0, z * 0 + outer - 1
    for _ in range(outer):
        take_left = z - left_end > right_end - z
        owner_z = jnp.where(take_left, left_end, right_end)
        order.append(lax.rem(z - owner_z + outer, outer))
        left_end = jnp.where(take_left, left_end + 1, left_end)
        right_end = jnp.where(take_left, right_end, right_end - 1)

    for o in order:
        compute(o)
    for o in order[:-1]:
        add(o)
    gather(0)
    pl.when(low)(lambda: far_arrived(0, -1))
    pl.when(high)(lambda: far_arrived(outer, 1))

    def total(ends):
        def chunk(r, carry):
            at = pl.multiple_of(r * 16, 16)
            value = part[pl.ds(at, 16), :].astype(jnp.float32)
            for i in range(1, inner):
                value += got[pl.ds(pl.multiple_of(i * rows + at, 16), 16), :].astype(jnp.float32)
            for end in ends:
                value += far[pl.ds(pl.multiple_of(end * rows + at, 16), 16), :].astype(jnp.float32)
            served[pl.ds(at, 16), :] = value.astype(jnp.bfloat16)
            return carry

        lax.fori_loop(0, rows // 16, chunk, 0)

    pl.when(low & high)(lambda: total((0, outer)))
    pl.when(low & jnp.logical_not(high))(lambda: total((0,)))
    pl.when(jnp.logical_not(low) & high)(lambda: total((outer,)))
    pl.when(jnp.logical_not(low | high))(lambda: total(()))

    for o, step, when in hops:
        pl.when(when)(lambda o=o, step=step: hop(o, step).wait_send())
    for n in range(inner, shards):
        if n % inner:
            block = block_of(tok, n)
            rdma(block, block, tok_send.at[n], tok_recv.at[n], ahead(0, n % inner)).wait_send()
    for o in range(1, outer):
        far_copy(o).wait_send()
    for copy in sends:
        copy.wait_send()

    def end_up(j, carry):
        mine, here, remote = up_copy(j)
        pl.when(jnp.logical_not(mine))(remote.wait_send)
        return carry

    lax.fori_loop(0, nseg, end_up, 0)
    for sg in range(groups):
        def end(sg=sg):
            whole = up_group(g, sg)
            for c in range(1, cores):
                rdma(whole, whole, tu_send.at[sg, 0, c], tu_recv.at[sg, 0],
                     to("tp", t, cores, c)).wait_send()
            for d in range(1, groups):
                def left(k, carry):
                    block = up_block(lax.rem(g + groups - d, groups), lax.rem(f + shards - k, shards), sg)
                    for c in range(1, cores):
                        rdma(block, block, ou_send.at[sg, d, c, k], ou_recv.at[sg, d, k],
                             to("tp", t, cores, c)).wait_send()
                    return carry

                lax.fori_loop(0, shards, left, 0)

        pl.when(owner(sg) == t)(end)


def body(tokens, norm_gain, up_weight, down_weight):
    groups, shards, cores = (lax.axis_size(a) for a in ("gr", "fs", "tp"))
    segment = down_weight.shape[0]
    up = (norm_gain[:, None] * up_weight).astype(jnp.bfloat16)
    down = down_weight.astype(jnp.bfloat16)
    values = tokens.astype(jnp.float32)
    normed = (values * lax.rsqrt(jnp.mean(values * values, axis=1, keepdims=True) + 1e-06)).astype(
        jnp.bfloat16
    )
    rows, depth = tokens.shape
    inner = inner_size(shards)
    nseg = up.shape[1] // segment
    width = groups * segment
    bf = jnp.bfloat16
    dma = pltpu.SemaphoreType.DMA
    vmem = pl.BlockSpec(memory_space=pltpu.VMEM)
    return pl.pallas_call(
        functools.partial(kernel, (groups, shards, cores)),
        out_shape=(
            jax.ShapeDtypeStruct((rows, depth), bf),
            jax.ShapeDtypeStruct((depth, width), bf),
            jax.ShapeDtypeStruct((width, depth), bf),
        ),
        in_specs=[vmem] * 3,
        out_specs=(vmem, vmem, vmem),
        scratch_shapes=[
            pltpu.VMEM((shards * rows, depth), bf),
            pltpu.VMEM((inner * rows, width), bf),
            pltpu.VMEM((shards * rows, depth), bf),
            pltpu.VMEM((shards * rows, depth), bf),
            pltpu.VMEM(((shards // inner + 1) * rows, depth), bf),
            dma((nseg,)), dma((groups, shards)),
            dma((groups, groups, shards)), dma((groups, groups, shards)),
            dma((groups, groups, cores)), dma((groups, groups)),
            dma((groups,)), dma((groups,)),
            dma((cores, groups)), dma((cores, groups)),
            dma((shards,)), dma((shards,)),
            dma((shards,)), dma((shards,)),
            dma((shards // inner,)), dma((shards // inner + 1,)), dma((2 * (shards // inner),)),
            dma((groups, groups, cores, shards)), dma((groups, groups, shards)),
            dma((2,)),
        ],
        compiler_params=pltpu.CompilerParams(
            collective_id=0, has_side_effects=True, vmem_limit_bytes=34 * 1024 * 1024
        ),
        name="serve",
    )(normed, up, down)


def solution(mesh):
    return jax.shard_map(
        body,
        mesh=mesh,
        in_specs=(
            P(("gr", "fs", "tp"), None),
            P(("gr", "fs")),
            P(("gr", "fs"), "tp"),
            P(("gr", "fs"), "tp"),
        ),
        out_specs=(P(("gr", "fs", "tp"), None), P(None, "fs"), P("fs", None)),
        check_vma=False,
    )
```

profile of v0, /device:TPU:10, one launch (start us, length us, event | category | flops | bytes accessed | tf_op | source)
XLA Modules:
  0.0 134.1 jit_solution(2029954313726395260)
XLA Ops:
  0.6 1.2 fusion
  1.9 0.0 copy-start
  1.9 1.3 %fusion.1.normed = bf16[128,2048]{1,0:T(8,128)(2,1)S(1)} fusion(bf16[128,2048]{1,0:T(8,128)(2,1)} %param.4, f32[128]{0:T(128)S(1)} %add_rsqrt_fusion), kind=kLoop, calls=%fused_computation.4 | loop fusion | flops 786432 | bytes 1049088 | tf_op jit(solution)/shard_map/convert_element_type | solution.py:381
  3.2 1.8 %multiply_convert_fusion.up = bf16[128,4096]{1,0:T(8,128)(2,1)S(1)} fusion(f32[128,4096]{1,0:T(8,128)} %param.6, f32[128]{0:T(128)} %param.5), kind=kLoop, calls=%fused_computation | loop fusion | flops 1048576 | bytes 3146240 | tf_op jit(solution)/shard_map/convert_element_type | solution.py:378
  5.0 0.0 copy-done
  5.1 0.2 convert_element_type.15.down
  5.2 124.0 %serve.1 = (bf16[128,2048]{1,0:T(8,128)(2,1)S(1)}, bf16[2048,1024]{1,0:T(8,128)(2,1)S(1)}, bf16[1024,2048]{1,0:T(8,128)(2,1)S(1)}) custom-call(bf16[128,2048]{1,0:T(8,128)(2,1)S(1)} %fusion.1.normed, bf16[128,4096]{1,0:T(8,128)(2,1)S(1)} %multiply_convert_fusion.up, bf16[512,1024]{1,0:T(8,128)(2,1)S(1)} %convert_element_type.15.down), custom_call_target="tpu_custom_call" | custom-call | tf_op jit(solution)/shard_map/serve/pallas_call | solution.py:391
  129.3 0.8 copy.10
  130.1 2.0 %copy.11 = bf16[2048,1024]{1,0:T(8,128)(2,1)} copy(bf16[2048,1024]{1,0:T(8,128)(2,1)S(1)} %get-tuple-element.7) | data formatting | bytes 8388608
  132.1 2.0 %copy.12 = bf16[1024,2048]{1,0:T(8,128)(2,1)} copy(bf16[1024,2048]{1,0:T(8,128)(2,1)S(1)} %get-tuple-element.8) | data formatting | bytes 8388608
  (1 shorter events, 0.0 us)
Async XLA Ops:
  1.9 3.2 %copy-start = (f32[512,1024]{1,0:T(8,128)S(1)}, f32[512,1024]{1,0:T(8,128)}, u32[]{:S(2)}) copy-start(f32[512,1024]{1,0:T(8,128)} %param.7) | copy-start | bytes 6291460
where the time goes:
time: 136 us; the launch traced here: 134 us
  Pallas kernels  124 us (91%)
  local copies, waits for them, and re-layouts  4.82 us (4%)
  other arithmetic  4.54 us (3%)
    pallas_call x1, Pallas kernels, body(): pl.pallas_call(functools.partial(kernel, (groups, shards, cores)), out_sh...  124 us
    unnamed x5, local copies, waits for them, and re-layouts  4.82 us

commit v1 on v0

v1 whole, which is shorter than its diff:
```python
import functools

import jax
import jax.numpy as jnp
from jax import lax
from jax.experimental import pallas as pl
from jax.experimental.pallas import tpu as pltpu
from jax.sharding import PartitionSpec as P

MESH = pl.DeviceIdType.MESH
TILE = 512
STEP = 16


def inner_size(shards):
    return max(d for d in range(1, shards + 1) if shards % d == 0 and d * d <= shards)


def heavy_rows(rows, inner):
    return rows if inner == 1 else max(STEP, rows * 3 // 4 // STEP * STEP)


def kernel(sizes, normed, up, down, served, su, sd, tok, hid, part, got, far, lit, rest, *sems):
    groups, shards, cores = sizes
    inner = inner_size(shards)
    outer = shards // inner
    (up_send, up_recv, gu_send, gu_recv, tu_send, tu_recv, gd_send, gd_recv,
     td_send, td_recv, hop_send, hop_recv, light_send, light_recv, heavy_send, heavy_recv,
     near_send, near_recv, far_send, far_recv, lit_send, lit_recv, ou_send, ou_recv, local) = sems
    g, f, t = lax.axis_index("gr"), lax.axis_index("fs"), lax.axis_index("tp")
    z, y = f // inner, lax.rem(f, inner)
    rows, depth = normed.shape
    own_rows = up.shape[0]
    segment, dcols = down.shape
    nseg = up.shape[1] // segment
    group_rows = shards * own_rows
    width = su.shape[1]
    heavy = heavy_rows(rows, inner)
    light = rows - heavy
    front = rows + (inner - 1) * light
    stack = inner * rows
    half = rows // 2
    tiles = depth // TILE
    low, high = z > 0, z < outer - 1

    def to(axis, me, size, step):
        return {axis: lax.rem(me + step, size)}

    def rdma(src, dst, send, recv, device):
        return pltpu.make_async_remote_copy(
            src_ref=src, dst_ref=dst, send_sem=send, recv_sem=recv,
            device_id=device, device_id_type=MESH,
        )

    def back(i):
        return {"fs": z * inner + lax.rem(y + inner - i, inner)}

    def ahead(i):
        return {"fs": z * inner + lax.rem(y + i, inner)}

    def beside(step):
        return {"fs": (z + step) * inner + y}

    def span(ref, start, count, n=None):
        at = pl.ds(start if isinstance(start, int) else pl.multiple_of(start, STEP), count)
        if n is None:
            return ref.at[at]
        return ref.at[at, pl.ds(n * TILE if isinstance(n, int) else pl.multiple_of(n * TILE, TILE), TILE)]

    peers = [to("fs", f, shards, k) for k in range(1, shards)]
    peers += [to("gr", g, groups, k) for k in range(1, groups)]
    peers += [to("tp", t, cores, k) for k in range(1, cores)]
    barrier = pltpu.get_barrier_semaphore()
    for peer in peers:
        pl.semaphore_signal(barrier, inc=1, device_id=peer, device_id_type=MESH)
    pl.semaphore_wait(barrier, len(peers))

    def up_block(group, shard, sg):
        row = pl.multiple_of((group * shards + shard) * own_rows, own_rows)
        return su.at[pl.ds(row, own_rows), pl.ds(pl.multiple_of(sg * segment, segment), segment)]

    def up_group(group, sg):
        row = pl.multiple_of(group * group_rows, group_rows)
        return su.at[pl.ds(row, group_rows), pl.ds(sg * segment, segment)]

    def down_block(group, core):
        row = pl.multiple_of(group * segment, segment)
        return sd.at[pl.ds(row, segment), pl.ds(pl.multiple_of(core * dcols, dcols), dcols)]

    def owner(sg):
        return (sg * shards + f) // nseg

    sends = []

    def begin(copy):
        copy.start()
        sends.append(copy)

    down_in = []
    for k in range(1, groups):
        begin(rdma(down, down_block(g, t), gd_send.at[k], gd_recv.at[k], to("gr", g, groups, k)))
        down_in.append((k, lax.rem(g + groups - k, groups)))

    def up_copy(i):
        number = t * nseg + i
        shard, sg = lax.rem(number, shards), number // shards
        step = lax.rem(shard - f + shards, shards)
        src = up.at[:, pl.ds(pl.multiple_of(i * segment, segment), segment)]
        remote = rdma(src, up_block(g, f, sg), up_send.at[i], up_recv.at[sg, step], {"fs": shard})
        here = pltpu.make_async_copy(src, up_block(g, f, sg), up_recv.at[sg, 0])
        return shard == f, here, remote

    def start_up(j, carry):
        mine, here, remote = up_copy(lax.rem(f + j, nseg))
        pl.when(mine)(here.start)
        pl.when(jnp.logical_not(mine))(remote.start)
        return carry

    lax.fori_loop(0, nseg, start_up, 0)

    keep_down = pltpu.make_async_copy(down, down_block(g, t), local.at[0])
    keep_tok = pltpu.make_async_copy(normed, span(tok, 0, rows), local.at[1])
    keep_down.start()
    keep_tok.start()

    pieces = [(0, half), (half, rows - half)] + ([(rows, front - rows)] if front > rows else [])

    def hop(o, step, c):
        start, count = pieces[c]
        n = o + step
        own = o in (0, outer)
        src = span(normed, start, count) if own and c < 2 else span(tok, (o % outer) * stack + start, count)
        index = n if step > 0 else outer + n
        return rdma(src, span(tok, n * stack + start, count), hop_send.at[index, c], hop_recv.at[n, c], beside(step))

    hops = []

    def move(o, step, c, when):
        pl.when(when)(lambda: hop(o, step, c).start())
        hops.append((o, step, c, when))

    def light_copy(i):
        return rdma(span(normed, heavy, light), span(tok, rows + (i - 1) * light, light),
                    light_send.at[i], light_recv.at[i], ahead(i))

    def heavy_copy(n, i, c):
        start = 0 if c == 0 else half
        count = min(half, heavy) if c == 0 else heavy - half
        src = span(normed, start, count) if isinstance(n, int) and n == 0 else span(tok, n * stack + start, count)
        return rdma(src, span(tok, n * stack + front + (i - 1) * heavy + start, count),
                    heavy_send.at[n, i, c], heavy_recv.at[n, i, c], ahead(i))

    parts = (0, 1) if heavy > half else (0,)

    if light:
        for i in range(1, inner):
            begin(light_copy(i))
    for c in range(2):
        if outer > 1:
            move(0, 1, c, high)
            move(outer, -1, c, low)
    for c in parts:
        for i in range(1, inner):
            begin(heavy_copy(0, i, c))
    for k in range(1, cores):
        begin(rdma(down, down_block(g, t), td_send.at[k, 0], td_recv.at[k, 0], to("tp", t, cores, k)))

    for sg in range(groups):
        def forward(sg=sg):
            def arrived(k, carry):
                shard = lax.rem(f + shards - k, shards)
                block = up_block(g, shard, sg)

                @pl.when(k == 0)
                def _():
                    pltpu.make_async_copy(block, block, up_recv.at[sg, 0]).wait()

                @pl.when(k > 0)
                def _():
                    rdma(block, block, up_send.at[0], up_recv.at[sg, k], {"fs": shard}).wait_recv()

                for d in range(1, groups):
                    rdma(block, block, gu_send.at[sg, d, k], gu_recv.at[sg, d, k],
                         to("gr", g, groups, d)).start()
                return carry

            lax.fori_loop(0, shards, arrived, 0)
            whole = up_group(g, sg)
            for c in range(1, cores):
                rdma(whole, whole, tu_send.at[sg, 0, c], tu_recv.at[sg, 0], to("tp", t, cores, c)).start()

        pl.when(owner(sg) == t)(forward)

    if light:
        for i in range(1, inner):
            light_copy(i).wait_recv()
        if outer > 1:
            move(0, 1, 2, high)
            move(outer, -1, 2, low)

    def pass_on(o):
        for c in range(len(pieces)):
            for n, when, step, more in ((o, z >= o, 1, high), (outer - o, z + o < outer, -1, low)):
                start, count = pieces[c]
                block = span(tok, n * stack + start, count)

                @pl.when(when)
                def _(n=n, step=step, block=block, c=c):
                    rdma(block, block, hop_send.at[0, c], hop_recv.at[n, c], beside(-step)).wait_recv()

                if 0 < n + step < outer:
                    move(n, step, c, when & more)

                if c in parts:
                    @pl.when(when)
                    def _(n=n, c=c):
                        for i in range(1, inner):
                            heavy_copy(n, i, c).start()

    if outer > 1:
        pass_on(1)

    for k, source in down_in:
        block = down_block(source, t)
        rdma(block, block, gd_send.at[k], gd_recv.at[k], {"gr": source}).wait_recv()
        for c in range(1, cores):
            begin(rdma(block, block, td_send.at[c, k], td_recv.at[c, k], to("tp", t, cores, c)))

    def onward(first, last):
        for sg in range(groups):
            def relay(sg=sg):
                for d in range(1, groups):
                    source = lax.rem(g + groups - d, groups)

                    def arrived(k, carry):
                        block = up_block(source, lax.rem(f + shards - k, shards), sg)
                        rdma(block, block, gu_send.at[sg, d, k], gu_recv.at[sg, d, k], {"gr": source}).wait()
                        for c in range(1, cores):
                            rdma(block, block, ou_send.at[sg, d, c, k], ou_recv.at[sg, d, k],
                                 to("tp", t, cores, c)).start()
                        return carry

                    lax.fori_loop(first, last, arrived, 0)

            pl.when(owner(sg) == t)(relay)

    onward(0, shards // 2)
    if outer > 2:
        pass_on(2)
    early = outer == 4
    if not early:
        for o in range(3, outer):
            pass_on(o)
    onward(shards // 2, shards)

    keep_down.wait()
    keep_tok.wait()
    for c in range(1, cores):
        core = lax.rem(t + cores - c, cores)
        for k in range(groups):
            block = down_block(lax.rem(g + groups - k, groups), core)
            rdma(block, block, td_send.at[c, k], td_recv.at[c, k], {"tp": core}).wait_recv()
    for sg in range(groups):
        def take(sg=sg):
            whole = up_group(g, sg)
            rdma(whole, whole, tu_send.at[sg, 0, 1], tu_recv.at[sg, 0], {"tp": owner(sg)}).wait_recv()
            for d in range(1, groups):
                def taken(k, carry):
                    block = up_block(lax.rem(g + groups - d, groups), lax.rem(f + shards - k, shards), sg)
                    rdma(block, block, tu_send.at[sg, 0, 1], ou_recv.at[sg, d, k],
                         {"tp": owner(sg)}).wait_recv()
                    return carry

                lax.fori_loop(0, shards, taken, 0)

        pl.when(owner(sg) != t)(take)

    def near_copy(o, i, n):
        return rdma(span(part, o * stack + front + (i - 1) * heavy, heavy, n),
                    span(got, (o * (inner - 1) + i - 1) * heavy, heavy, n),
                    near_send.at[o, i, n], near_recv.at[o, i, n], back(i))

    def far_copy(o, n):
        right = o > z
        step = jnp.where(right, 1, -1)
        last = jnp.where(right, o == outer - 1, o == 1)
        slot = jnp.where(last, jnp.where(right, 0, outer), o + step)
        return rdma(span(part, o * stack, front, n), span(far, slot * front, front, n),
                    far_send.at[o, n], far_recv.at[slot, n], beside(step))

    def far_arrived(slot, step, n):
        block = span(far, slot * front, front, n)
        rdma(block, block, far_send.at[0, 0], far_recv.at[slot, n], beside(step)).wait_recv()

    def clear(slot):
        def zero(r, carry):
            far[pl.ds(pl.multiple_of(slot * front + r * STEP, STEP), STEP), :] = jnp.zeros((STEP, depth), jnp.bfloat16)
            return carry

        lax.fori_loop(0, front // STEP, zero, 0)

    def passes(o):
        right = o > z
        return (right & low) | (jnp.logical_not(right) & high)

    for o in range(1, outer):
        pl.when(jnp.logical_not(passes(o)))(lambda o=o: clear(o))
    pl.when(jnp.logical_not(low))(lambda: clear(0))
    pl.when(jnp.logical_not(high))(lambda: clear(outer))

    def compute(o):
        for i in range(1, inner):
            for c in parts:
                start = 0 if c == 0 else half
                count = min(half, heavy) if c == 0 else heavy - half
                block = span(tok, o * stack + front + (i - 1) * heavy + start, count)
                rdma(block, block, heavy_send.at[o, i, c], heavy_recv.at[o, i, c], back(i)).wait_recv()
        both = pl.ds(pl.multiple_of(o * stack, stack), stack)

        def first(n, carry):
            cols = pl.ds(pl.multiple_of(n * TILE, TILE), TILE)
            product = jnp.dot(tok[both, :], su[:, cols], preferred_element_type=jnp.float32)
            product = jnp.maximum(product, 0.0)
            hid[:, cols] = (product * product).astype(jnp.bfloat16)
            return carry

        lax.fori_loop(0, width // TILE, first, 0)

        def second(n, carry):
            cols = pl.ds(pl.multiple_of(n * TILE, TILE), TILE)
            product = jnp.dot(hid[...], sd[:, cols], preferred_element_type=jnp.float32)
            part[both, cols] = product.astype(jnp.bfloat16)
            for i in range(1, inner):
                near_copy(o, i, n).start()
            return carry

        lax.fori_loop(0, tiles, second, 0)

    def gather(o, n):
        for i in range(1, inner):
            near_copy(o, i, n).wait()

    def cells(start, n):
        return pl.ds(pl.multiple_of(start, STEP), STEP), pl.ds(pl.multiple_of(n * TILE, TILE), TILE)

    def value_at(o, r, n, ends, spread):
        value = part[cells(o * stack + r * STEP, n)].astype(jnp.float32)
        if spread:
            for i in range(1, inner):
                value += got[cells((o * (inner - 1) + i - 1) * heavy + r * STEP, n)].astype(jnp.float32)
        for end in ends:
            value += far[cells(end * front + r * STEP, n)].astype(jnp.float32)
        return value

    def add(o):
        def tile(n, carry):
            gather(o, n)

            @pl.when(passes(o))
            def _():
                far_arrived(o, jnp.where(o > z, -1, 1), n)

            def chunk(spread, r, carry):
                value = value_at(o, r, n, (o,), spread)
                part[cells(o * stack + r * STEP, n)] = value.astype(jnp.bfloat16)
                return carry

            lax.fori_loop(0, heavy // STEP, functools.partial(chunk, True), 0)
            lax.fori_loop(heavy // STEP, front // STEP, functools.partial(chunk, False), 0)
            far_copy(o, n).start()
            return carry

        lax.fori_loop(0, tiles, tile, 0)

    order = []
    left_end, right_end = z * 0, z * 0 + outer - 1
    for _ in range(outer):
        take_left = z - left_end > right_end - z
        owner_z = jnp.where(take_left, left_end, right_end)
        order.append(lax.rem(z - owner_z + outer, outer))
        left_end = jnp.where(take_left, left_end + 1, left_end)
        right_end = jnp.where(take_left, right_end, right_end - 1)
    if early:
        second_far, first_far, third_far, _ = order
        compute(first_far)
        compute(third_far)
        add(first_far)
        pass_on(3)
        compute(second_far)
        add(second_far)
        compute(0)
        add(third_far)
    else:
        for o in order[:-1]:
            compute(o)
        compute(0)
        for o in order[:-1]:
            add(o)

    def lit_copy(i, n):
        return rdma(span(part, rows + (i - 1) * light, light, n), span(lit, (i - 1) * light, light, n),
                    lit_send.at[i, n], lit_recv.at[i, n], back(i))

    def total(n, carry):
        gather(0, n)
        pl.when(low)(lambda: far_arrived(0, -1, n))
        pl.when(high)(lambda: far_arrived(outer, 1, n))
        ends = (0, outer)

        def others(r, carry):
            part[cells(r * STEP, n)] = value_at(0, r, n, ends, False).astype(jnp.bfloat16)
            return carry

        def half_done(r, carry):
            rest[cells((r * STEP - heavy), n)] = value_at(0, r, n, ends, False)
            return carry

        def done(r, carry):
            served[cells(r * STEP, n)] = value_at(0, r, n, ends, True).astype(jnp.bfloat16)
            return carry

        if light:
            lax.fori_loop(rows // STEP, front // STEP, others, 0)
            for i in range(1, inner):
                lit_copy(i, n).start()
            lax.fori_loop(heavy // STEP, rows // STEP, half_done, 0)
        lax.fori_loop(0, heavy // STEP, done, 0)
        return carry

    lax.fori_loop(0, tiles, total, 0)

    if light:
        def finish(n, carry):
            for i in range(1, inner):
                lit_copy(i, n).wait()

            def chunk(r, carry):
                value = rest[cells(r * STEP, n)]
                for i in range(1, inner):
                    value += lit[cells((i - 1) * light + r * STEP, n)].astype(jnp.float32)
                served[cells(heavy + r * STEP, n)] = value.astype(jnp.bfloat16)
                return carry

            lax.fori_loop(0, light // STEP, chunk, 0)
            return carry

        lax.fori_loop(0, tiles, finish, 0)

    for o, step, c, when in hops:
        pl.when(when)(lambda o=o, step=step, c=c: hop(o, step, c).wait_send())
    for n in range(1, outer):
        for c in parts:
            for i in range(1, inner):
                heavy_copy(n, i, c).wait_send()

        def gone(m, carry, n=n):
            far_copy(n, m).wait_send()
            return carry

        lax.fori_loop(0, tiles, gone, 0)
    for copy in sends:
        copy.wait_send()

    def end_up(j, carry):
        mine, here, remote = up_copy(j)
        pl.when(jnp.logical_not(mine))(remote.wait_send)
        return carry

    lax.fori_loop(0, nseg, end_up, 0)
    for sg in range(groups):
        def end(sg=sg):
            whole = up_group(g, sg)
            for c in range(1, cores):
                rdma(whole, whole, tu_send.at[sg, 0, c], tu_recv.at[sg, 0],
                     to("tp", t, cores, c)).wait_send()
            for d in range(1, groups):
                def left(k, carry):
                    block = up_block(lax.rem(g + groups - d, groups), lax.rem(f + shards - k, shards), sg)
                    for c in range(1, cores):
                        rdma(block, block, ou_send.at[sg, d, c, k], ou_recv.at[sg, d, k],
                             to("tp", t, cores, c)).wait_send()
                    return carry

                lax.fori_loop(0, shards, left, 0)

        pl.when(owner(sg) == t)(end)


def body(tokens, norm_gain, up_weight, down_weight):
    groups, shards, cores = (lax.axis_size(a) for a in ("gr", "fs", "tp"))
    segment = down_weight.shape[0]
    up = (norm_gain[:, None] * up_weight).astype(jnp.bfloat16)
    down = down_weight.astype(jnp.bfloat16)
    values = tokens.astype(jnp.float32)
    normed = (values * lax.rsqrt(jnp.mean(values * values, axis=1, keepdims=True) + 1e-06)).astype(
        jnp.bfloat16
    )
    rows, depth = tokens.shape
    inner = inner_size(shards)
    outer = shards // inner
    heavy = heavy_rows(rows, inner)
    light = rows - heavy
    front = rows + (inner - 1) * light
    nseg = up.shape[1] // segment
    width = groups * segment
    tiles = depth // TILE
    bf = jnp.bfloat16
    dma = pltpu.SemaphoreType.DMA
    vmem = pl.BlockSpec(memory_space=pltpu.VMEM)
    return pl.pallas_call(
        functools.partial(kernel, (groups, shards, cores)),
        out_shape=(
            jax.ShapeDtypeStruct((rows, depth), bf),
            jax.ShapeDtypeStruct((depth, width), bf),
            jax.ShapeDtypeStruct((width, depth), bf),
        ),
        in_specs=[vmem] * 3,
        out_specs=(vmem, vmem, vmem),
        scratch_shapes=[
            pltpu.VMEM((shards * rows, depth), bf),
            pltpu.VMEM((inner * rows, width), bf),
            pltpu.VMEM((shards * rows, depth), bf),
            pltpu.VMEM((max(outer * (inner - 1) * heavy, STEP), depth), bf),
            pltpu.VMEM(((outer + 1) * front, depth), bf),
            pltpu.VMEM((max((inner - 1) * light, STEP), depth), bf),
            pltpu.VMEM((max(light, STEP), depth), jnp.float32),
            dma((nseg,)), dma((groups, shards)),
            dma((groups, groups, shards)), dma((groups, groups, shards)),
            dma((groups, groups, cores)), dma((groups, groups)),
            dma((groups,)), dma((groups,)),
            dma((cores, groups)), dma((cores, groups)),
            dma((2 * outer, 3)), dma((outer, 3)),
            dma((inner,)), dma((inner,)),
            dma((outer, inner, 2)), dma((outer, inner, 2)),
            dma((outer, inner, tiles)), dma((outer, inner, tiles)),
            dma((outer, tiles)), dma((outer + 1, tiles)),
            dma((inner, tiles)), dma((inner, tiles)),
            dma((groups, groups, cores, shards)), dma((groups, groups, shards)),
            dma((2,)),
        ],
        compiler_params=pltpu.CompilerParams(
            collective_id=0, has_side_effects=True, vmem_limit_bytes=40 * 1024 * 1024
        ),
        name="serve",
    )(normed, up, down)


def solution(mesh):
    return jax.shard_map(
        body,
        mesh=mesh,
        in_specs=(
            P(("gr", "fs", "tp"), None),
            P(("gr", "fs")),
            P(("gr", "fs"), "tp"),
            P(("gr", "fs"), "tp"),
        ),
        out_specs=(P(("gr", "fs", "tp"), None), P(None, "fs"), P("fs", None)),
        check_vma=False,
    )
```

time: 136 us -> 159 us (1.17); the launches traced: 134 us -> 159 us
  Pallas kernels: 124 us -> 149 us
    pallas_call x1, Pallas kernels: 124 us -> 149 us  [body(): pl.pallas_call(functools.partial(kernel, (groups, shards, cores)), out_sh...]
where the time goes in v1:
time: 159 us
  Pallas kernels  149 us (94%)
  local copies, waits for them, and re-layouts  4.82 us (3%)
  other arithmetic  4.54 us (3%)
    pallas_call x1, Pallas kernels, body(): pl.pallas_call(functools.partial(kernel, (groups, shards, cores)), out_sh...  149 us
    unnamed x5, local copies, waits for them, and re-layouts  4.82 us

profile of v1, /device:TPU:10, one launch (start us, length us, event | category | flops | bytes accessed | tf_op | source)
XLA Modules:
  0.0 158.9 jit_solution(14544578626880513488)
XLA Ops:
  0.6 1.2 fusion
  1.9 0.0 copy-start
  1.9 1.3 fusion.1.normed
  3.2 1.8 %multiply_convert_fusion.up = bf16[128,4096]{1,0:T(8,128)(2,1)S(1)} fusion(f32[128,4096]{1,0:T(8,128)} %param.6, f32[128]{0:T(128)} %param.5), kind=kLoop, calls=%fused_computation | loop fusion | flops 1048576 | bytes 3146240 | tf_op jit(solution)/shard_map/convert_element_type | solution.py:492
  5.0 0.0 copy-done
  5.1 0.2 convert_element_type.15.down
  5.2 148.8 %serve.1 = (bf16[128,2048]{1,0:T(8,128)(2,1)S(1)}, bf16[2048,1024]{1,0:T(8,128)(2,1)S(1)}, bf16[1024,2048]{1,0:T(8,128)(2,1)S(1)}) custom-call(bf16[128,2048]{1,0:T(8,128)(2,1)S(1)} %fusion.1.normed, bf16[128,4096]{1,0:T(8,128)(2,1)S(1)} %multiply_convert_fusion.up, bf16[512,1024]{1,0:T(8,128)(2,1)S(1)} %convert_element_type.15.down), custom_call_target="tpu_custom_call" | custom-call | tf_op jit(solution)/shard_map/serve/pallas_call | solution.py:510
  154.0 0.8 copy.10
  154.8 2.0 %copy.11 = bf16[2048,1024]{1,0:T(8,128)(2,1)} copy(bf16[2048,1024]{1,0:T(8,128)(2,1)S(1)} %get-tuple-element.7) | data formatting | bytes 8388608
  156.9 2.0 %copy.12 = bf16[1024,2048]{1,0:T(8,128)(2,1)} copy(bf16[1024,2048]{1,0:T(8,128)(2,1)S(1)} %get-tuple-element.8) | data formatting | bytes 8388608
  (1 shorter events, 0.0 us)
Async XLA Ops:
  1.9 3.2 %copy-start = (f32[512,1024]{1,0:T(8,128)S(1)}, f32[512,1024]{1,0:T(8,128)}, u32[]{:S(2)}) copy-start(f32[512,1024]{1,0:T(8,128)} %param.7) | copy-start | bytes 6291460

commit v2 on v1

v2 whole, which is shorter than its diff:
```python
import functools

import jax
import jax.numpy as jnp
from jax import lax
from jax.experimental import pallas as pl
from jax.experimental.pallas import tpu as pltpu
from jax.sharding import PartitionSpec as P

MESH = pl.DeviceIdType.MESH
TILE = 512
STEP = 16
LAG = 2


def inner_size(shards):
    return max(d for d in range(1, shards + 1) if shards % d == 0 and d * d <= shards)


def heavy_rows(rows, inner):
    return rows if inner == 1 else max(STEP, rows * 3 // 4 // STEP * STEP)


def kernel(sizes, tokens, gain, up_in, down_in, served, su, sd, tok, hid, part, got, far, lit, rest,
           raw, scale, wide_up, wide_down, up, *sems):
    groups, shards, cores = sizes
    inner = inner_size(shards)
    outer = shards // inner
    (up_send, up_recv, gu_send, gu_recv, tu_send, tu_recv, gd_send, gd_recv,
     td_send, td_recv, hop_send, hop_recv, light_send, light_recv, heavy_send, heavy_recv,
     near_send, near_recv, far_send, far_recv, lit_send, lit_recv, ou_send, ou_recv, load, load_up, ou_down_send, ou_down_recv) = sems
    g, f, t = lax.axis_index("gr"), lax.axis_index("fs"), lax.axis_index("tp")
    z, y = f // inner, lax.rem(f, inner)
    rows, depth = raw.shape
    own_rows = up.shape[0]
    segment, dcols = wide_down.shape
    nseg = up.shape[1] // segment
    group_rows = shards * own_rows
    width = su.shape[1]
    heavy = heavy_rows(rows, inner)
    light = rows - heavy
    front = rows + (inner - 1) * light
    stack = inner * rows
    half = rows // 2
    tile = min(TILE, dcols)
    tiles = depth // tile
    cuts = dcols // tile
    low, high = z > 0, z < outer - 1
    middle, end = low & high, jnp.logical_not(low & high)
    near_low = 2 * z < outer - 1
    inward = jnp.where(near_low, 1, -1)

    def to(axis, me, size, step):
        return {axis: lax.rem(me + step, size)}

    def rdma(src, dst, send, recv, device):
        return pltpu.make_async_remote_copy(
            src_ref=src, dst_ref=dst, send_sem=send, recv_sem=recv,
            device_id=device, device_id_type=MESH,
        )

    def back(i):
        return {"fs": z * inner + lax.rem(y + inner - i, inner)}

    def ahead(i):
        return {"fs": z * inner + lax.rem(y + i, inner)}

    def beside(step):
        return {"fs": (z + step) * inner + y}

    def span(ref, start, count, n=None):
        at = pl.ds(start if isinstance(start, int) else pl.multiple_of(start, STEP), count)
        if n is None:
            return ref.at[at]
        return ref.at[at, pl.ds(n * tile if isinstance(n, int) else pl.multiple_of(n * tile, tile), tile)]

    peers = [to("fs", f, shards, k) for k in range(1, shards)]
    peers += [to("gr", g, groups, k) for k in range(1, groups)]
    peers += [to("tp", t, cores, k) for k in range(1, cores)]
    def up_block(group, shard, sg):
        row = pl.multiple_of((group * shards + shard) * own_rows, own_rows)
        return su.at[pl.ds(row, own_rows), pl.ds(pl.multiple_of(sg * segment, segment), segment)]

    def up_group(group, sg):
        row = pl.multiple_of(group * group_rows, group_rows)
        return su.at[pl.ds(row, group_rows), pl.ds(sg * segment, segment)]

    def down_block(group, core):
        row = pl.multiple_of(group * segment, segment)
        return sd.at[pl.ds(row, segment), pl.ds(pl.multiple_of(core * dcols, dcols), dcols)]

    def down_piece(group, core, q):
        row = pl.multiple_of(group * segment, segment)
        return sd.at[pl.ds(row, segment), pl.ds(pl.multiple_of(core * dcols + q * tile, tile), tile)]

    def owner(sg):
        return (sg * shards + f) // nseg

    sends = []

    def begin(copy):
        copy.start()
        sends.append(copy)

    def listed(j, away):
        r, i = j // inner, lax.rem(j, inner)
        rows_z = [z] + [jnp.where(middle, z + a * inward, z + b * inward)
                        for a, b in zip(away, (1, 2, 3))] if outer == 4 else [
                            lax.rem(z + d, outer) for d in range(outer)]
        at = rows_z[0]
        for d in range(1, outer):
            at = jnp.where(r == d, rows_z[d], at)
        return at * inner + lax.rem(y + i, inner)

    loads = [pltpu.make_async_copy(down_in, wide_down, load.at[0]),
             pltpu.make_async_copy(gain, scale, load.at[1]),
             pltpu.make_async_copy(tokens, raw, load.at[2])]

    def load_segment(i):
        cols = pl.ds(pl.multiple_of(i * segment, segment), segment)
        return pltpu.make_async_copy(up_in.at[:, cols], wide_up.at[:, cols], load_up.at[i])

    def target(j):
        return listed(nseg - 1 - j, (-1, 1, 2)) if nseg == shards else lax.rem(f + j, nseg)

    def start_load(j, carry):
        load_segment(target(j)).start()
        return carry

    for copy in loads:
        copy.start()
    lax.fori_loop(0, nseg, start_load, 0)

    barrier = pltpu.get_barrier_semaphore()
    for peer in peers:
        pl.semaphore_signal(barrier, inc=1, device_id=peer, device_id_type=MESH)

    loads[0].wait()

    def round_down(r, carry):
        row = pl.multiple_of(r * STEP, STEP)
        sd[pl.ds(pl.multiple_of(g * segment + row, STEP), STEP), pl.ds(pl.multiple_of(t * dcols, dcols), dcols)] = (
            wide_down[pl.ds(row, STEP), :].astype(jnp.bfloat16))
        return carry

    lax.fori_loop(0, segment // STEP, round_down, 0)
    loads[2].wait()

    def norm(r, carry):
        at = pl.ds(pl.multiple_of(r * STEP, STEP), STEP)
        value = raw[at, :].astype(jnp.float32)
        inverse = lax.rsqrt(jnp.mean(value * value, axis=1, keepdims=True) + 1e-06)
        tok[at, :] = (value * inverse).astype(jnp.bfloat16)
        return carry

    lax.fori_loop(0, rows // STEP, norm, 0)

    loads[1].wait()
    shape = (own_rows, own_rows)
    diagonal = lax.broadcasted_iota(jnp.int32, shape, 0) == lax.broadcasted_iota(jnp.int32, shape, 1)
    column = jnp.sum(jnp.where(diagonal, scale[...], 0.0), axis=1, keepdims=True)
    pl.semaphore_wait(barrier, len(peers))

    def down_copy(k, q):
        block = down_piece(g, t, q)
        return rdma(block, block, gd_send.at[k, q], gd_recv.at[k, q], to("gr", g, groups, k))

    def down_sent(q):
        for k in range(1, groups):
            begin(down_copy(k, q))

    early_cuts = max(1, cuts // 2)
    for q in range(early_cuts):
        down_sent(q)

    pieces = [(0, half), (half, rows - half)] + ([(rows, front - rows)] if front > rows else [])

    def apart(distance):
        low_way, high_way = outer - distance, distance
        return jnp.where(near_low, low_way, high_way), jnp.where(near_low, high_way, low_way)

    def hop(o, way, c):
        start, count = pieces[c]
        step = -inward if way else inward
        n = lax.rem(o + step + outer, outer)
        return rdma(span(tok, o * stack + start, count), span(tok, n * stack + start, count),
                    hop_send.at[o, way, c], hop_recv.at[n, c], beside(step))

    parts = (0, 1) if heavy > half else (0,)
    hops = []

    def move(o, way, which, when):
        for c in which:
            if c < len(pieces):
                pl.when(when)(lambda c=c: hop(o, way, c).start())
                hops.append((o, way, c, when))

    def arrive(o, which, when, way=None):
        for c in which:
            if c < len(pieces):
                start, count = pieces[c]

                @pl.when(when)
                def _(c=c, start=start, count=count):
                    block = span(tok, o * stack + start, count)
                    rdma(block, block, hop_send.at[0, 0, c], hop_recv.at[o, c], beside(0 * z + inward)).wait_recv()

                if way is not None:
                    move(o, way, (c,), when)
                if c in parts:
                    @pl.when(when)
                    def _(c=c):
                        for i in range(1, inner):
                            heavy_copy(o, i, c).start()

    def light_copy(i):
        return rdma(span(tok, heavy, light), span(tok, rows + (i - 1) * light, light),
                    light_send.at[i], light_recv.at[i], ahead(i))

    def heavy_copy(n, i, c):
        start = 0 if c == 0 else half
        count = min(half, heavy) if c == 0 else heavy - half
        src = span(tok, n * stack + start, count)
        return rdma(src, span(tok, n * stack + front + (i - 1) * heavy + start, count),
                    heavy_send.at[n, i, c], heavy_recv.at[n, i, c], ahead(i))


    def up_copy(i):
        number = t * nseg + i
        shard, sg = lax.rem(number, shards), number // shards
        step = lax.rem(shard - f + shards, shards)
        src = up.at[:, pl.ds(pl.multiple_of(i * segment, segment), segment)]
        remote = rdma(src, up_block(g, f, sg), up_send.at[i], up_recv.at[sg, step], {"fs": shard})
        return shard == f, sg, remote

    def start_up(j, carry):
        i = target(j)
        mine, sg, remote = up_copy(i)
        load_segment(i).wait()
        cols = pl.ds(pl.multiple_of(i * segment, segment), segment)
        value = (wide_up[:, cols] * column).astype(jnp.bfloat16)
        up[:, cols] = value

        @pl.when(mine)
        def _():
            row = pl.multiple_of((g * shards + f) * own_rows, own_rows)
            su[pl.ds(row, own_rows), pl.ds(pl.multiple_of(sg * segment, segment), segment)] = value

        pl.when(jnp.logical_not(mine))(remote.start)
        return carry

    zero = z * 0
    in_one, out_one = apart(1)
    if outer > 1:
        move(zero, 0, (0,), z >= 0)
        move(zero, 1, (0,), middle)
    lax.fori_loop(0, nseg, start_up, 0)
    if light:
        for i in range(1, inner):
            begin(light_copy(i))
    if outer > 1:
        move(zero, 0, (1,), z >= 0)
        move(zero, 1, (1,), middle)
    for c in parts:
        for i in range(1, inner):
            begin(heavy_copy(0, i, c))
    for k in range(1, cores):
        block = down_block(g, t)
        begin(rdma(block, block, ou_down_send.at[k], ou_down_recv.at[k], to("tp", t, cores, k)))

    def forward(first, last):
        def of_segment(sg):
            def arrived(j, carry):
                shard = listed(j, (2, -1, 1))
                k = lax.rem(f - shard + shards, shards)
                block = up_block(g, shard, sg)

                @pl.when(k > 0)
                def _():
                    rdma(block, block, up_send.at[0], up_recv.at[sg, k], {"fs": shard}).wait_recv()

                for d in range(1, groups):
                    rdma(block, block, gu_send.at[sg, d, k], gu_recv.at[sg, d, k],
                         to("gr", g, groups, d)).start()
                return carry

            lax.fori_loop(first, last, arrived, 0)
            if last == shards:
                whole = up_group(g, sg)
                for c in range(1, cores):
                    rdma(whole, whole, tu_send.at[sg, 0, c], tu_recv.at[sg, 0], to("tp", t, cores, c)).start()

        for sg in range(groups):
            pl.when(owner(sg) == t)(lambda sg=sg: of_segment(sg))

    forward(0, inner)
    if light:
        for i in range(1, inner):
            light_copy(i).wait_recv()
        if outer > 1:
            move(zero, 0, (2,), z >= 0)
    if outer == 4:
        pl.when(end)(lambda: forward(inner, 2 * inner))
        in_two, in_three = apart(2)[0], apart(3)[0]
        arrive(out_one, (0,), middle, 0)
        arrive(in_one, (0,), middle, 1)
        arrive(in_one, (0,), end)
    if outer == 4:
        pl.when(middle)(lambda: forward(inner, 2 * inner))
    forward(2 * inner if outer == 4 else inner, shards)

    if outer == 4:
        order = [jnp.where(middle, a, b) for a, b in
                 ((in_one, in_two), (out_one, in_three), (in_two, in_one), (zero, zero))]
        arrive(out_one, (1, 2), middle, 0)
        arrive(in_one, (1,), middle, 1)
        arrive(order[0], (2,), middle, 1)
        arrive(in_one, (1,), end)
        arrive(in_two, (0,), end)
        for q in range(early_cuts, cuts):
            down_sent(q)
        arrive(in_two, (1,), end)

    def down_on(q):
        for k in range(1, groups):
            source = lax.rem(g + groups - k, groups)
            block = down_piece(source, t, q)
            rdma(block, block, gd_send.at[k, q], gd_recv.at[k, q], {"gr": source}).wait_recv()
            for c in range(1, cores):
                begin(rdma(block, block, td_send.at[c, k, q], td_recv.at[c, k, q], to("tp", t, cores, c)))

    def down_here(q):
        for c in range(1, cores):
            core = lax.rem(t + cores - c, cores)
            for k in range(1, groups):
                block = down_piece(lax.rem(g + groups - k, groups), core, q)
                rdma(block, block, td_send.at[c, k, q], td_recv.at[c, k, q], {"tp": core}).wait_recv()

    for q in range(early_cuts):
        down_on(q)

    for sg in range(groups):
        def relay(sg=sg):
            for d in range(1, groups):
                source = lax.rem(g + groups - d, groups)

                def arrived(j, carry):
                    shard = listed(j, (2, -1, 1))
                    k = lax.rem(f - shard + shards, shards)
                    block = up_block(source, shard, sg)
                    rdma(block, block, gu_send.at[sg, d, k], gu_recv.at[sg, d, k], {"gr": source}).wait()
                    for c in range(1, cores):
                        rdma(block, block, ou_send.at[sg, d, c, k], ou_recv.at[sg, d, k],
                             to("tp", t, cores, c)).start()
                    return carry

                lax.fori_loop(0, shards, arrived, 0)

        pl.when(owner(sg) == t)(relay)

    for c in range(1, cores):
        core = lax.rem(t + cores - c, cores)
        block = down_block(g, core)
        rdma(block, block, ou_down_send.at[c], ou_down_recv.at[c], {"tp": core}).wait_recv()
    for sg in range(groups):
        def take(sg=sg):
            whole = up_group(g, sg)
            rdma(whole, whole, tu_send.at[sg, 0, 1], tu_recv.at[sg, 0], {"tp": owner(sg)}).wait_recv()
            for d in range(1, groups):
                def taken(k, carry):
                    block = up_block(lax.rem(g + groups - d, groups), lax.rem(f + shards - k, shards), sg)
                    rdma(block, block, tu_send.at[sg, 0, 1], ou_recv.at[sg, d, k],
                         {"tp": owner(sg)}).wait_recv()
                    return carry

                lax.fori_loop(0, shards, taken, 0)

        pl.when(owner(sg) != t)(take)

    def near_copy(o, i, n):
        return rdma(span(part, o * stack + front + (i - 1) * heavy, heavy, n),
                    span(got, (o * (inner - 1) + i - 1) * heavy, heavy, n),
                    near_send.at[o, i, n], near_recv.at[o, i, n], back(i))

    def far_copy(o, n):
        right = o > z
        step = jnp.where(right, 1, -1)
        last = jnp.where(right, o == outer - 1, o == 1)
        slot = jnp.where(last, jnp.where(right, 0, outer), o + step)
        return rdma(span(part, o * stack, front, n), span(far, slot * front, front, n),
                    far_send.at[o, n], far_recv.at[slot, n], beside(step))

    def far_arrived(slot, step, n):
        block = span(far, slot * front, front, n)
        rdma(block, block, far_send.at[0, 0], far_recv.at[slot, n], beside(step)).wait_recv()

    def clear(slot):
        def zero(r, carry):
            far[pl.ds(pl.multiple_of(slot * front + r * STEP, STEP), STEP), :] = jnp.zeros((STEP, depth), jnp.bfloat16)
            return carry

        lax.fori_loop(0, front // STEP, zero, 0)

    def passes(o):
        right = o > z
        return (right & low) | (jnp.logical_not(right) & high)

    pl.when(jnp.logical_not(low))(lambda: clear(0))
    pl.when(jnp.logical_not(high))(lambda: clear(outer))

    def tile_of(s):
        return lax.rem(s, cores) * cuts + s // cores

    def hide(o):
        for i in range(1, inner):
            for c in parts:
                start = 0 if c == 0 else half
                count = min(half, heavy) if c == 0 else heavy - half
                block = span(tok, o * stack + front + (i - 1) * heavy + start, count)
                rdma(block, block, heavy_send.at[o, i, c], heavy_recv.at[o, i, c], back(i)).wait_recv()
        both = pl.ds(pl.multiple_of(o * stack, stack), stack)

        def first(n, carry):
            cols = pl.ds(pl.multiple_of(n * TILE, TILE), TILE)
            product = jnp.dot(tok[both, :], su[:, cols], preferred_element_type=jnp.float32)
            product = jnp.maximum(product, 0.0)
            hid[:, cols] = (product * product).astype(jnp.bfloat16)
            return carry

        lax.fori_loop(0, width // TILE, first, 0)

    def project(o, start, stop):
        both = pl.ds(pl.multiple_of(o * stack, stack), stack)

        def second(s, carry):
            n = tile_of(s)
            cols = pl.ds(pl.multiple_of(n * tile, tile), tile)
            product = jnp.dot(hid[...], sd[:, cols], preferred_element_type=jnp.float32)
            part[both, cols] = product.astype(jnp.bfloat16)
            for i in range(1, inner):
                near_copy(o, i, n).start()
            return carry

        lax.fori_loop(start, stop, second, 0)

    def compute(o):
        hide(o)
        project(o, 0, tiles)

    def gather(o, n):
        for i in range(1, inner):
            near_copy(o, i, n).wait()

    def cells(start, n):
        return pl.ds(pl.multiple_of(start, STEP), STEP), pl.ds(pl.multiple_of(n * tile, tile), tile)

    def value_at(o, r, n, ends, spread):
        value = part[cells(o * stack + r * STEP, n)].astype(jnp.float32)
        if spread:
            for i in range(1, inner):
                value += got[cells((o * (inner - 1) + i - 1) * heavy + r * STEP, n)].astype(jnp.float32)
        for end in ends:
            value += far[cells(end * front + r * STEP, n)].astype(jnp.float32)
        return value

    def add_tile(o, n):
        gather(o, n)

        def sums(ends):
            def chunk(spread, r, carry):
                value = value_at(o, r, n, ends, spread)
                part[cells(o * stack + r * STEP, n)] = value.astype(jnp.bfloat16)
                return carry

            lax.fori_loop(0, heavy // STEP, functools.partial(chunk, True), 0)
            if ends:
                lax.fori_loop(heavy // STEP, front // STEP, functools.partial(chunk, False), 0)

        @pl.when(passes(o))
        def _():
            far_arrived(o, jnp.where(o > z, -1, 1), n)
            sums((o,))

        pl.when(jnp.logical_not(passes(o)))(lambda: sums(()))
        far_copy(o, n).start()

    def add(first, then, start, stop):
        lag = 0 if then is None else LAG

        def tile_sums(s, carry):
            pl.when(s < stop)(lambda: add_tile(first, tile_of(s)))
            if then is not None:
                pl.when(middle & (s >= start + lag))(lambda: add_tile(then, tile_of(s - lag)))
            return carry

        lax.fori_loop(start, stop + lag, tile_sums, 0)

    ready = early_cuts * cores
    if outer == 4:
        for q in range(early_cuts):
            down_here(q)
        arrive(order[0], (2,), end)
        arrive(in_two, (0,), middle, 1)
        hide(order[0])
        project(order[0], 0, ready)
        arrive(in_three, (0,), end)
        pl.when(end)(lambda: add(order[0], None, 0, ready))
        arrive(in_two, (1, 2), middle, 1)
        move(zero, 1, (2,), middle)
        for q in range(early_cuts, cuts):
            down_on(q)
        for q in range(early_cuts, cuts):
            down_here(q)
        project(order[0], ready, tiles)
        arrive(in_three, (1,), end)
        pl.when(end)(lambda: add(order[0], None, ready, tiles))
        arrive(in_three, (2,), end)
        compute(order[1])

        @pl.when(middle)
        def _():
            compute(order[2])
            compute(order[3])
            add(order[0], None, 0, tiles)

        arrive(in_one, (2,), end)
        pl.when(end)(lambda: compute(order[2]))
        add(jnp.where(middle, in_two, in_three), out_one, 0, tiles)

        @pl.when(end)
        def _():
            compute(order[3])
            add(order[2], None, 0, tiles)

    else:
        raise NotImplementedError("rows along z")

    def lit_copy(i, n):
        return rdma(span(part, rows + (i - 1) * light, light, n), span(lit, (i - 1) * light, light, n),
                    lit_send.at[i, n], lit_recv.at[i, n], back(i))

    def total(s, carry):
        n = tile_of(s)
        gather(0, n)
        pl.when(low)(lambda: far_arrived(0, -1, n))
        pl.when(high)(lambda: far_arrived(outer, 1, n))
        ends = (0, outer)

        def others(r, carry):
            part[cells(r * STEP, n)] = value_at(0, r, n, ends, False).astype(jnp.bfloat16)
            return carry

        def half_done(r, carry):
            rest[cells((r * STEP - heavy), n)] = value_at(0, r, n, ends, False)
            return carry

        def done(r, carry):
            served[cells(r * STEP, n)] = value_at(0, r, n, ends, True).astype(jnp.bfloat16)
            return carry

        if light:
            lax.fori_loop(rows // STEP, front // STEP, others, 0)
            for i in range(1, inner):
                lit_copy(i, n).start()
            lax.fori_loop(heavy // STEP, rows // STEP, half_done, 0)
        lax.fori_loop(0, heavy // STEP, done, 0)
        return carry

    lax.fori_loop(0, tiles, total, 0)

    if light:
        def finish(s, carry):
            n = tile_of(s)

            for i in range(1, inner):
                lit_copy(i, n).wait()

            def chunk(r, carry):
                value = rest[cells(r * STEP, n)]
                for i in range(1, inner):
                    value += lit[cells((i - 1) * light + r * STEP, n)].astype(jnp.float32)
                served[cells(heavy + r * STEP, n)] = value.astype(jnp.bfloat16)
                return carry

            lax.fori_loop(0, light // STEP, chunk, 0)
            return carry

        lax.fori_loop(0, tiles, finish, 0)

    for o, way, c, when in hops:
        pl.when(when)(lambda o=o, way=way, c=c: hop(o, way, c).wait_send())
    for n in range(1, outer):
        for c in parts:
            for i in range(1, inner):
                heavy_copy(n, i, c).wait_send()

        def gone(m, carry, n=n):
            far_copy(n, m).wait_send()
            return carry

        lax.fori_loop(0, tiles, gone, 0)
    for copy in sends:
        copy.wait_send()

    def end_up(j, carry):
        mine, sg, remote = up_copy(j)
        pl.when(jnp.logical_not(mine))(remote.wait_send)
        return carry

    lax.fori_loop(0, nseg, end_up, 0)
    for sg in range(groups):
        def end(sg=sg):
            whole = up_group(g, sg)
            for c in range(1, cores):
                rdma(whole, whole, tu_send.at[sg, 0, c], tu_recv.at[sg, 0],
                     to("tp", t, cores, c)).wait_send()
            for d in range(1, groups):
                def left(k, carry):
                    block = up_block(lax.rem(g + groups - d, groups), lax.rem(f + shards - k, shards), sg)
                    for c in range(1, cores):
                        rdma(block, block, ou_send.at[sg, d, c, k], ou_recv.at[sg, d, k],
                             to("tp", t, cores, c)).wait_send()
                    return carry

                lax.fori_loop(0, shards, left, 0)

        pl.when(owner(sg) == t)(end)


def body(tokens, norm_gain, up_weight, down_weight):
    groups, shards, cores = (lax.axis_size(a) for a in ("gr", "fs", "tp"))
    segment = down_weight.shape[0]
    rows, depth = tokens.shape
    inner = inner_size(shards)
    outer = shards // inner
    heavy = heavy_rows(rows, inner)
    light = rows - heavy
    front = rows + (inner - 1) * light
    own_rows, columns = up_weight.shape
    nseg = columns // segment
    width = groups * segment
    dcols = down_weight.shape[1]
    tile = min(TILE, dcols)
    tiles = depth // tile
    cuts = dcols // tile
    bf = jnp.bfloat16
    dma = pltpu.SemaphoreType.DMA
    vmem = pl.BlockSpec(memory_space=pltpu.VMEM)
    return pl.pallas_call(
        functools.partial(kernel, (groups, shards, cores)),
        out_shape=(
            jax.ShapeDtypeStruct((rows, depth), bf),
            jax.ShapeDtypeStruct((depth, width), bf),
            jax.ShapeDtypeStruct((width, depth), bf),
        ),
        in_specs=[pl.BlockSpec(memory_space=pltpu.HBM)] * 4,
        out_specs=(vmem, vmem, vmem),
        scratch_shapes=[
            pltpu.VMEM((shards * rows, depth), bf),
            pltpu.VMEM((inner * rows, width), bf),
            pltpu.VMEM((shards * rows, depth), bf),
            pltpu.VMEM((max(outer * (inner - 1) * heavy, STEP), depth), bf),
            pltpu.VMEM(((outer + 1) * front, depth), bf),
            pltpu.VMEM((max((inner - 1) * light, STEP), depth), bf),
            pltpu.VMEM((max(light, STEP), depth), jnp.float32),
            pltpu.VMEM((rows, depth), bf),
            pltpu.VMEM((1, own_rows), jnp.float32),
            pltpu.VMEM((own_rows, columns), jnp.float32),
            pltpu.VMEM((segment, dcols), jnp.float32),
            pltpu.VMEM((own_rows, columns), bf),
            dma((nseg,)), dma((groups, shards)),
            dma((groups, groups, shards)), dma((groups, groups, shards)),
            dma((groups, groups, cores)), dma((groups, groups)),
            dma((groups, cuts)), dma((groups, cuts)),
            dma((cores, groups, cuts)), dma((cores, groups, cuts)),
            dma((outer, 2, 3)), dma((outer, 3)),
            dma((inner,)), dma((inner,)),
            dma((outer, inner, 2)), dma((outer, inner, 2)),
            dma((outer, inner, tiles)), dma((outer, inner, tiles)),
            dma((outer, tiles)), dma((outer + 1, tiles)),
            dma((inner, tiles)), dma((inner, tiles)),
            dma((groups, groups, cores, shards)), dma((groups, groups, shards)),
            dma((3,)), dma((nseg,)), dma((cores,)), dma((cores,)),
        ],
        compiler_params=pltpu.CompilerParams(
            collective_id=0, has_side_effects=True, vmem_limit_bytes=40 * 1024 * 1024
        ),
        name="serve",
    )(*(pltpu.with_memory_space_constraint(a, pltpu.HBM) for a in (tokens, norm_gain[None, :], up_weight, down_weight)))


def solution(mesh):
    return jax.shard_map(
        body,
        mesh=mesh,
        in_specs=(
            P(("gr", "fs", "tp"), None),
            P(("gr", "fs")),
            P(("gr", "fs"), "tp"),
            P(("gr", "fs"), "tp"),
        ),
        out_specs=(P(("gr", "fs", "tp"), None), P(None, "fs"), P("fs", None)),
        check_vma=False,
    )
```

time: 159 us -> 121 us (0.76)
  Pallas kernels: 149 us -> 115 us
  other arithmetic: 4.54 us -> 0 us
    pallas_call x1, Pallas kernels: 149 us -> 115 us  [body(): pl.pallas_call(functools.partial(kernel, (groups, shards, cores)), out_sh...]
    convert_element_type x3 -> x0, other arithmetic: 3.31 us -> none  [the longest x1 1.81 us: body(): up = (norm_gain[:, None] * up_weight).astype(jnp.bfloat16)]
    unnamed x5 -> x3, local copies, waits for them, and re-layouts: 4.82 us -> 4.82 us
where the time goes in v2:
time: 121 us; the launch traced here: 120 us
  Pallas kernels  115 us (95%)
  local copies, waits for them, and re-layouts  4.82 us (4%)
    pallas_call x1, Pallas kernels, body(): pl.pallas_call(functools.partial(kernel, (groups, shards, cores)), out_sh...  115 us
    unnamed x3, local copies, waits for them, and re-layouts  4.82 us

profile of v2, /device:TPU:10, one launch (start us, length us, event | category | flops | bytes accessed | tf_op | source)
XLA Modules:
  0.0 120.0 jit_solution(2229736119105079562)
XLA Ops:
  0.6 114.5 %serve.1 = (bf16[128,2048]{1,0:T(8,128)(2,1)S(1)}, bf16[2048,1024]{1,0:T(8,128)(2,1)S(1)}, bf16[1024,2048]{1,0:T(8,128)(2,1)S(1)}) custom-call(bf16[128,2048]{1,0:T(8,128)(2,1)} %tokens.1, f32[1,128]{1,0:T(1,128)} %bitcast.1, f32[128,4096]{1,0:T(8,128)} %up_in.1, f32[512,1024]{1,0:T(8,128)} %down_in.1), custom_call_target="tpu_custom_call" | custom-call | tf_op jit(solution)/shard_map/serve/pallas_call | solution.py:649
  115.2 0.8 copy.10
  116.0 2.0 %copy.11 = bf16[2048,1024]{1,0:T(8,128)(2,1)} copy(bf16[2048,1024]{1,0:T(8,128)(2,1)S(1)} %get-tuple-element.7) | data formatting | bytes 8388608
  118.0 2.0 %copy.12 = bf16[1024,2048]{1,0:T(8,128)(2,1)} copy(bf16[1024,2048]{1,0:T(8,128)(2,1)S(1)} %get-tuple-element.8) | data formatting | bytes 8388608

commit v3 on v2

--- a/solution.py
+++ b/solution.py
@@ -10,7 +10,9 @@
 MESH = pl.DeviceIdType.MESH
 TILE = 512
 STEP = 16
-LAG = 2
+LAG = 1
+BEHIND = 2
+HEAVY = 6
 
 
 def inner_size(shards):
@@ -18,7 +20,7 @@
 
 
 def heavy_rows(rows, inner):
-    return rows if inner == 1 else max(STEP, rows * 3 // 4 // STEP * STEP)
+    return rows * HEAVY // 8 // STEP * STEP
 
 
 def kernel(sizes, tokens, gain, up_in, down_in, served, su, sd, tok, hid, part, got, far, lit, rest,
@@ -102,11 +104,12 @@
         copy.start()
         sends.append(copy)
 
-    def listed(j, away):
+    def listed(j, middle_rows, end_rows):
         r, i = j // inner, lax.rem(j, inner)
-        rows_z = [z] + [jnp.where(middle, z + a * inward, z + b * inward)
-                        for a, b in zip(away, (1, 2, 3))] if outer == 4 else [
-                            lax.rem(z + d, outer) for d in range(outer)]
+        if outer == 4:
+            rows_z = [jnp.where(middle, z + a * inward, z + b * inward) for a, b in zip(middle_rows, end_rows)]
+        else:
+            rows_z = [lax.rem(z + d, outer) for d in range(outer)]
         at = rows_z[0]
         for d in range(1, outer):
             at = jnp.where(r == d, rows_z[d], at)
@@ -121,7 +124,7 @@
         return pltpu.make_async_copy(up_in.at[:, cols], wide_up.at[:, cols], load_up.at[i])
 
     def target(j):
-        return listed(nseg - 1 - j, (-1, 1, 2)) if nseg == shards else lax.rem(f + j, nseg)
+        return listed(j, (2, -1, 0, 1), (3, 2, 0, 1)) if nseg == shards else lax.rem(f + j, nseg)
 
     def start_load(j, carry):
         load_segment(target(j)).start()
@@ -173,7 +176,7 @@
     for q in range(early_cuts):
         down_sent(q)
 
-    pieces = [(0, half), (half, rows - half)] + ([(rows, front - rows)] if front > rows else [])
+    pieces = [(0, half), (half, heavy - half), (heavy, front - heavy)]
 
     def apart(distance):
         low_way, high_way = outer - distance, distance
@@ -186,7 +189,7 @@
         return rdma(span(tok, o * stack + start, count), span(tok, n * stack + start, count),
                     hop_send.at[o, way, c], hop_recv.at[n, c], beside(step))
 
-    parts = (0, 1) if heavy > half else (0,)
+    parts = (0, 1)
     hops = []
 
     def move(o, way, which, when):
@@ -251,16 +254,16 @@
 
     zero = z * 0
     in_one, out_one = apart(1)
-    if outer > 1:
-        move(zero, 0, (0,), z >= 0)
-        move(zero, 1, (0,), middle)
-    lax.fori_loop(0, nseg, start_up, 0)
+    first_part = inner if nseg == shards else nseg
+    last_part = shards - inner if nseg == shards else nseg
+    move(zero, 0, (0,), z >= 0)
     if light:
         for i in range(1, inner):
             begin(light_copy(i))
-    if outer > 1:
-        move(zero, 0, (1,), z >= 0)
-        move(zero, 1, (1,), middle)
+    lax.fori_loop(0, first_part, start_up, 0)
+    move(zero, 0, (1,), middle)
+    lax.fori_loop(first_part, last_part, start_up, 0)
+    move(zero, 1, (0,), middle)
     for c in parts:
         for i in range(1, inner):
             begin(heavy_copy(0, i, c))
@@ -268,10 +271,15 @@
         block = down_block(g, t)
         begin(rdma(block, block, ou_down_send.at[k], ou_down_recv.at[k], to("tp", t, cores, k)))
 
+    def down_rest():
+        for q in range(early_cuts, cuts):
+            for k in range(1, groups):
+                down_copy(k, q).start()
+
     def forward(first, last):
         def of_segment(sg):
             def arrived(j, carry):
-                shard = listed(j, (2, -1, 1))
+                shard = listed(j, (0, 2, -1, 1), (0, 1, 2, 3))
                 k = lax.rem(f - shard + shards, shards)
                 block = up_block(g, shard, sg)
 
@@ -293,32 +301,37 @@
         for sg in range(groups):
             pl.when(owner(sg) == t)(lambda sg=sg: of_segment(sg))
 
-    forward(0, inner)
+    forward(0, 1)
     if light:
         for i in range(1, inner):
             light_copy(i).wait_recv()
-        if outer > 1:
-            move(zero, 0, (2,), z >= 0)
+    move(zero, 0, (2,), middle)
+    lax.fori_loop(last_part, nseg, start_up, 0)
+    move(zero, 0, (1, 2), end)
+    forward(1, inner)
     if outer == 4:
-        pl.when(end)(lambda: forward(inner, 2 * inner))
+        pl.when(end)(lambda: forward(inner, shards))
         in_two, in_three = apart(2)[0], apart(3)[0]
         arrive(out_one, (0,), middle, 0)
         arrive(in_one, (0,), middle, 1)
         arrive(in_one, (0,), end)
     if outer == 4:
-        pl.when(middle)(lambda: forward(inner, 2 * inner))
-    forward(2 * inner if outer == 4 else inner, shards)
+        pl.when(middle)(lambda: forward(inner, 3 * inner))
+        pl.when(middle)(down_rest)
+    else:
+        forward(inner, shards)
 
     if outer == 4:
         order = [jnp.where(middle, a, b) for a, b in
-                 ((in_one, in_two), (out_one, in_three), (in_two, in_one), (zero, zero))]
-        arrive(out_one, (1, 2), middle, 0)
+                 ((in_one, in_two), (in_two, in_three), (out_one, in_one), (zero, zero))]
         arrive(in_one, (1,), middle, 1)
         arrive(order[0], (2,), middle, 1)
-        arrive(in_one, (1,), end)
+        move(zero, 1, (1,), middle)
+        arrive(out_one, (1, 2), middle, 0)
+        pl.when(middle)(lambda: forward(3 * inner, shards))
+        arrive(in_two, (0,), middle, 1)
         arrive(in_two, (0,), end)
-        for q in range(early_cuts, cuts):
-            down_sent(q)
+        pl.when(end)(down_rest)
         arrive(in_two, (1,), end)
 
     def down_on(q):
@@ -345,7 +358,7 @@
                 source = lax.rem(g + groups - d, groups)
 
                 def arrived(j, carry):
-                    shard = listed(j, (2, -1, 1))
+                    shard = listed(j, (0, 2, -1, 1), (0, 1, 2, 3))
                     k = lax.rem(f - shard + shards, shards)
                     block = up_block(source, shard, sg)
                     rdma(block, block, gu_send.at[sg, d, k], gu_recv.at[sg, d, k], {"gr": source}).wait()
@@ -495,16 +508,30 @@
 
         lax.fori_loop(start, stop + lag, tile_sums, 0)
 
+    def beside_sums(o, later):
+        def step(s, carry):
+            pl.when(s < tiles)(lambda: add_tile(o, tile_of(s)))
+            pl.when(s >= BEHIND)(lambda: project(later, s - BEHIND, s - BEHIND + 1))
+            return carry
+
+        lax.fori_loop(0, tiles + BEHIND, step, 0)
+
+    def wait_far():
+        def gone(s, carry):
+            far_copy(in_three, tile_of(s)).wait_send()
+            return carry
+
+        lax.fori_loop(0, tiles - 1, gone, 0)
+
     ready = early_cuts * cores
     if outer == 4:
         for q in range(early_cuts):
             down_here(q)
         arrive(order[0], (2,), end)
-        arrive(in_two, (0,), middle, 1)
         hide(order[0])
         project(order[0], 0, ready)
+        arrive(in_one, (1,), end)
         arrive(in_three, (0,), end)
-        pl.when(end)(lambda: add(order[0], None, 0, ready))
         arrive(in_two, (1, 2), middle, 1)
         move(zero, 1, (2,), middle)
         for q in range(early_cuts, cuts):
@@ -513,24 +540,28 @@
             down_here(q)
         project(order[0], ready, tiles)
         arrive(in_three, (1,), end)
+        pl.when(end)(lambda: add(order[0], None, 0, ready))
         pl.when(end)(lambda: add(order[0], None, ready, tiles))
         arrive(in_three, (2,), end)
         compute(order[1])
 
         @pl.when(middle)
         def _():
+            add(order[0], None, 0, tiles // 2)
             compute(order[2])
+            add(order[0], None, tiles // 2, tiles)
             compute(order[3])
-            add(order[0], None, 0, tiles)
+            add(in_two, out_one, 0, tiles)
 
         arrive(in_one, (2,), end)
-        pl.when(end)(lambda: compute(order[2]))
-        add(jnp.where(middle, in_two, in_three), out_one, 0, tiles)
 
         @pl.when(end)
         def _():
-            compute(order[3])
-            add(order[2], None, 0, tiles)
+            hide(order[2])
+            beside_sums(in_three, order[2])
+            hide(order[3])
+            wait_far()
+            beside_sums(order[2], order[3])
 
     else:
         raise NotImplementedError("rows along z")
@@ -595,12 +626,16 @@
                 heavy_copy(n, i, c).wait_send()
 
         def gone(m, carry, n=n):
-            far_copy(n, m).wait_send()
+            waited = end & (n == apart(3)[0]) & (m != tile_of(tiles - 1))
+            pl.when(jnp.logical_not(waited))(lambda: far_copy(n, m).wait_send())
             return carry
 
         lax.fori_loop(0, tiles, gone, 0)
     for copy in sends:
         copy.wait_send()
+    for q in range(early_cuts, cuts):
+        for k in range(1, groups):
+            down_copy(k, q).wait_send()
 
     def end_up(j, carry):
         mine, sg, remote = up_copy(j)

time: 121 us -> 116 us (0.959)
  Pallas kernels: 115 us -> 109 us
    pallas_call x1, Pallas kernels: 115 us -> 109 us  [body(): pl.pallas_call(functools.partial(kernel, (groups, shards, cores)), out_sh...]
where the time goes in v3:
time: 116 us; the launch traced here: 114 us
  Pallas kernels  109 us (94%)
  local copies, waits for them, and re-layouts  4.82 us (4%)
    pallas_call x1, Pallas kernels, body(): pl.pallas_call(functools.partial(kernel, (groups, shards, cores)), out_sh...  109 us
    unnamed x3, local copies, waits for them, and re-layouts  4.82 us

profile of v3, /device:TPU:10, one launch (start us, length us, event | category | flops | bytes accessed | tf_op | source)
XLA Modules:
  0.0 114.4 jit_solution(7863100222780687044)
XLA Ops:
  0.6 109.0 %serve.1 = (bf16[128,2048]{1,0:T(8,128)(2,1)S(1)}, bf16[2048,1024]{1,0:T(8,128)(2,1)S(1)}, bf16[1024,2048]{1,0:T(8,128)(2,1)S(1)}) custom-call(bf16[128,2048]{1,0:T(8,128)(2,1)} %tokens.1, f32[1,128]{1,0:T(1,128)} %bitcast.1, f32[128,4096]{1,0:T(8,128)} %up_in.1, f32[512,1024]{1,0:T(8,128)} %down_in.1), custom_call_target="tpu_custom_call" | custom-call | tf_op jit(solution)/shard_map/serve/pallas_call | solution.py:684
  109.6 0.8 copy.10
  110.4 2.0 %copy.11 = bf16[2048,1024]{1,0:T(8,128)(2,1)} copy(bf16[2048,1024]{1,0:T(8,128)(2,1)S(1)} %get-tuple-element.7) | data formatting | bytes 8388608
  112.4 2.0 %copy.12 = bf16[1024,2048]{1,0:T(8,128)(2,1)} copy(bf16[1024,2048]{1,0:T(8,128)(2,1)S(1)} %get-tuple-element.8) | data formatting | bytes 8388608

commit v4 on v3

--- a/solution.py
+++ b/solution.py
@@ -13,6 +13,7 @@
 LAG = 1
 BEHIND = 2
 HEAVY = 6
+CUTS = 2
 
 
 def inner_size(shards):
@@ -130,23 +131,14 @@
         load_segment(target(j)).start()
         return carry
 
-    for copy in loads:
-        copy.start()
+    for k in (2, 1, 0):
+        loads[k].start()
     lax.fori_loop(0, nseg, start_load, 0)
 
     barrier = pltpu.get_barrier_semaphore()
     for peer in peers:
         pl.semaphore_signal(barrier, inc=1, device_id=peer, device_id_type=MESH)
 
-    loads[0].wait()
-
-    def round_down(r, carry):
-        row = pl.multiple_of(r * STEP, STEP)
-        sd[pl.ds(pl.multiple_of(g * segment + row, STEP), STEP), pl.ds(pl.multiple_of(t * dcols, dcols), dcols)] = (
-            wide_down[pl.ds(row, STEP), :].astype(jnp.bfloat16))
-        return carry
-
-    lax.fori_loop(0, segment // STEP, round_down, 0)
     loads[2].wait()
 
     def norm(r, carry):
@@ -158,6 +150,15 @@
 
     lax.fori_loop(0, rows // STEP, norm, 0)
 
+    loads[0].wait()
+
+    def round_down(r, carry):
+        row = pl.multiple_of(r * STEP, STEP)
+        sd[pl.ds(pl.multiple_of(g * segment + row, STEP), STEP), pl.ds(pl.multiple_of(t * dcols, dcols), dcols)] = (
+            wide_down[pl.ds(row, STEP), :].astype(jnp.bfloat16))
+        return carry
+
+    lax.fori_loop(0, segment // STEP, round_down, 0)
     loads[1].wait()
     shape = (own_rows, own_rows)
     diagonal = lax.broadcasted_iota(jnp.int32, shape, 0) == lax.broadcasted_iota(jnp.int32, shape, 1)
@@ -528,11 +529,12 @@
         for q in range(early_cuts):
             down_here(q)
         arrive(order[0], (2,), end)
+        arrive(in_two, (1,), middle, 1)
         hide(order[0])
         project(order[0], 0, ready)
         arrive(in_one, (1,), end)
         arrive(in_three, (0,), end)
-        arrive(in_two, (1, 2), middle, 1)
+        arrive(in_two, (2,), middle, 1)
         move(zero, 1, (2,), middle)
         for q in range(early_cuts, cuts):
             down_on(q)
@@ -681,7 +683,7 @@
     bf = jnp.bfloat16
     dma = pltpu.SemaphoreType.DMA
     vmem = pl.BlockSpec(memory_space=pltpu.VMEM)
-    return pl.pallas_call(
+    served, su, sd = pl.pallas_call(
         functools.partial(kernel, (groups, shards, cores)),
         out_shape=(
             jax.ShapeDtypeStruct((rows, depth), bf),
@@ -722,6 +724,31 @@
         ),
         name="serve",
     )(*(pltpu.with_memory_space_constraint(a, pltpu.HBM) for a in (tokens, norm_gain[None, :], up_weight, down_weight)))
+    results = (served, su, sd)
+    return pl.pallas_call(
+        put_out,
+        out_shape=tuple(jax.ShapeDtypeStruct(a.shape, a.dtype) for a in results),
+        in_specs=[vmem] * 3,
+        out_specs=(pl.BlockSpec(memory_space=pltpu.HBM),) * 3,
+        scratch_shapes=[dma((3 * CUTS,))],
+        compiler_params=pltpu.CompilerParams(vmem_limit_bytes=1 * 1024 * 1024),
+        name="put_out",
+    )(*results)
+
+
+def put_out(*refs):
+    arrays, sem = refs[:-1], refs[-1]
+    half = len(arrays) // 2
+    copies = []
+    for src, dst in zip(arrays[:half], arrays[half:]):
+        count = src.shape[0] // CUTS
+        for c in range(CUTS):
+            at = pl.ds(c * count, count)
+            copies.append(pltpu.make_async_copy(src.at[at], dst.at[at], sem.at[len(copies)]))
+    for copy in copies:
+        copy.start()
+    for copy in copies:
+        copy.wait()
 
 
 def solution(mesh):

time: 116 us -> 113 us (0.974); the launches traced: 114 us -> 113 us
  local copies, waits for them, and re-layouts: 4.82 us -> 0 us
  Pallas kernels: 109 us -> 112 us
    unnamed x3 -> x0, local copies, waits for them, and re-layouts: 4.82 us -> none
    pallas_call x0 -> x1, Pallas kernels: none -> 3.56 us  [body(): pl.pallas_call(put_out, out_shape=tuple((jax.ShapeDtypeStruct(a.shape, a....]
where the time goes in v4:
time: 113 us
  Pallas kernels  112 us (99%)
    pallas_call x1, Pallas kernels, body(): pl.pallas_call(functools.partial(kernel, (groups, shards, cores)), out_sh...  109 us
    pallas_call x1, Pallas kernels, body(): pl.pallas_call(put_out, out_shape=tuple((jax.ShapeDtypeStruct(a.shape, a....  3.56 us

profile of v4, /device:TPU:10, one launch (start us, length us, event | category | flops | bytes accessed | tf_op | source)
XLA Modules:
  0.0 112.8 jit_solution(17577918457085405101)
XLA Ops:
  0.6 108.6 %serve.1 = (bf16[128,2048]{1,0:T(8,128)(2,1)S(1)}, bf16[2048,1024]{1,0:T(8,128)(2,1)S(1)}, bf16[1024,2048]{1,0:T(8,128)(2,1)S(1)}) custom-call(bf16[128,2048]{1,0:T(8,128)(2,1)} %tokens.1, f32[1,128]{1,0:T(1,128)} %bitcast.1, f32[128,4096]{1,0:T(8,128)} %up_in.1, f32[512,1024]{1,0:T(8,128)} %down_in.1), custom_call_target="tpu_custom_call" | custom-call | tf_op jit(solution)/shard_map/serve/pallas_call | solution.py:686
  109.2 3.6 %put_out.1 = (bf16[128,2048]{1,0:T(8,128)(2,1)}, bf16[2048,1024]{1,0:T(8,128)(2,1)}, bf16[1024,2048]{1,0:T(8,128)(2,1)}) custom-call(bf16[128,2048]{1,0:T(8,128)(2,1)S(1)} %get-tuple-element.6.refs_0_, bf16[2048,1024]{1,0:T(8,128)(2,1)S(1)} %get-tuple-element.7.refs_1_, bf16[1024,2048]{1,0:T(8,128)(2,1)S(1)} %get-tuple-element.8.refs_2_), custom_call_target="tpu_custom_call" | custom-call | tf_op jit(solution)/shard_map/put_out/pallas_call | solution.py:728

commit v5 on v4

--- a/solution.py
+++ b/solution.py
@@ -533,6 +533,7 @@
         hide(order[0])
         project(order[0], 0, ready)
         arrive(in_one, (1,), end)
+        pl.when(end)(lambda: add(order[0], None, 0, ready))
         arrive(in_three, (0,), end)
         arrive(in_two, (2,), middle, 1)
         move(zero, 1, (2,), middle)
@@ -542,7 +543,6 @@
             down_here(q)
         project(order[0], ready, tiles)
         arrive(in_three, (1,), end)
-        pl.when(end)(lambda: add(order[0], None, 0, ready))
         pl.when(end)(lambda: add(order[0], None, ready, tiles))
         arrive(in_three, (2,), end)
         compute(order[1])

time: 113 us -> 112 us (level)
  no operation moved by 1% of the time
where the time goes in v5:
time: 112 us
  Pallas kernels  111 us (99%)
    pallas_call x1, Pallas kernels, body(): pl.pallas_call(functools.partial(kernel, (groups, shards, cores)), out_sh...  108 us
    pallas_call x1, Pallas kernels, body(): pl.pallas_call(put_out, out_shape=tuple((jax.ShapeDtypeStruct(a.shape, a....  3.56 us

profile of v5, /device:TPU:10, one launch (start us, length us, event | category | flops | bytes accessed | tf_op | source)
XLA Modules:
  0.0 112.0 jit_solution(1926289825943587897)
XLA Ops:
  0.6 107.8 %serve.1 = (bf16[128,2048]{1,0:T(8,128)(2,1)S(1)}, bf16[2048,1024]{1,0:T(8,128)(2,1)S(1)}, bf16[1024,2048]{1,0:T(8,128)(2,1)S(1)}) custom-call(bf16[128,2048]{1,0:T(8,128)(2,1)} %tokens.1, f32[1,128]{1,0:T(1,128)} %bitcast.1, f32[128,4096]{1,0:T(8,128)} %up_in.1, f32[512,1024]{1,0:T(8,128)} %down_in.1), custom_call_target="tpu_custom_call" | custom-call | tf_op jit(solution)/shard_map/serve/pallas_call | solution.py:686
  108.4 3.6 %put_out.1 = (bf16[128,2048]{1,0:T(8,128)(2,1)}, bf16[2048,1024]{1,0:T(8,128)(2,1)}, bf16[1024,2048]{1,0:T(8,128)(2,1)}) custom-call(bf16[128,2048]{1,0:T(8,128)(2,1)S(1)} %get-tuple-element.6.refs_0_, bf16[2048,1024]{1,0:T(8,128)(2,1)S(1)} %get-tuple-element.7.refs_1_, bf16[1024,2048]{1,0:T(8,128)(2,1)S(1)} %get-tuple-element.8.refs_2_), custom_call_target="tpu_custom_call" | custom-call | tf_op jit(solution)/shard_map/put_out/pallas_call | solution.py:728
